TPU v7x, 512 devices: a whole 4x8x8 slice. The times are simulated.
512 devices in a mesh: ep: 32 (over z, x), tp: 16 (over y, core).
Axes of the slice: x: 4, y: 8, z: 8, core: 2. Of those that a mesh axis runs over, the one named last changes fastest.
Arguments:
- tokens: bfloat16 [16384, 4096], P('ep', 'tp'), may hold values from -6 to 6
- cotangent: bfloat16 [16384, 4096], P('ep', 'tp'), may hold values from -6 to 6
- expert_ids: int32 [16384, 2], P('ep'), may hold values from 0 to 63, as said below
- route_weight: float32 [16384, 2], P('ep'), may hold values from 0.1 to 1
- gate_weight: bfloat16 [64, 4096, 512], P('ep', 'tp'), may hold values from -0.09375 to 0.09375
- up_weight: bfloat16 [64, 4096, 512], P('ep', 'tp'), may hold values from -0.09375 to 0.09375
- down_weight: bfloat16 [64, 512, 4096], P('ep', None, 'tp'), may hold values from -0.25 to 0.25
- saved_gate: bfloat16 [32, 64, 32, 512], P(None, 'ep'), may hold values from -6 to 6
- saved_up: bfloat16 [32, 64, 32, 512], P(None, 'ep'), may hold values from -6 to 6
Outputs:
- token_grad: bfloat16 [16384, 4096], P('ep', 'tp')
- route_grad: float32 [16384, 2], P('ep')
- gate_weight_grad: bfloat16 [64, 4096, 512], P('ep', 'tp')
- up_weight_grad: bfloat16 [64, 4096, 512], P('ep', 'tp')
- down_weight_grad: bfloat16 [64, 512, 4096], P('ep', None, 'tp')
Inputs may be any that keep to these rules, and one draw needn't show every extreme that they name: `expert_ids`: each row names 2 different experts of one group of 4 consecutive experts. In each aligned block of 512 rows (the rows of one index of ep) no expert is named more than 32 times; the experts of one group, drawn from the seed, are named exactly 32 times in every block, and other experts may reach 32 too.
All inputs are finite; a program needn't handle non-finite values.
Results may differ from a plain program's by a relative error of at most 0.02.
Values may be sent and summed in bfloat16 or wider, within the bound.
A program may use at most 64 MiB of HBM per device.

v0:
```python
import jax
import jax.numpy as jnp
from jax import lax
from jax.sharding import Mesh
from jax.sharding import PartitionSpec as P

EP = ("ep_0", "ep_1")


def cut_along(x, dim, length):
    before, after = (x.shape[:dim], x.shape[dim + 1 :])
    return jnp.moveaxis(x.reshape(*before, length, -1, *after), dim, 0)


def laid_out(tiles, dim):
    lengths = list(tiles.shape[1:])
    lengths[dim] *= tiles.shape[0]
    return jnp.moveaxis(tiles, 0, dim).reshape(lengths)


def moved_by_axis(tiles, axes, order):
    lengths = [lax.axis_size(a) for a in axes]
    tiles = tiles.reshape(*lengths, *tiles.shape[1:])
    for k in order:
        tiles = lax.all_to_all(tiles, axes[k], split_axis=k, concat_axis=k, tiled=True)
    return tiles.reshape(-1, *tiles.shape[len(axes) :])


def stepwise_exchange(x, axes, order, split_dim, concat_dim):
    tiles = cut_along(x, split_dim, lax.axis_size(axes))
    return laid_out(moved_by_axis(tiles, axes, order), concat_dim)


def local(
    tokens,
    cotangent,
    expert_ids,
    route_weight,
    gate_weight,
    up_weight,
    down_weight,
    saved_gate,
    saved_up,
):
    sources = lax.axis_size(EP)
    tok_rows, width_local = tokens.shape
    top_k = expert_ids.shape[1]
    local_experts = gate_weight.shape[0]
    all_experts = local_experts * sources
    capacity = saved_gate.shape[2]
    assigned = tok_rows * top_k
    flat_ids = expert_ids.reshape(-1)
    onehot = (flat_ids[:, None] == jnp.arange(all_experts, dtype=jnp.int32)[None, :]).astype(
        jnp.int32
    )
    earlier = jnp.cumsum(onehot, axis=0) - onehot
    slot_index = jnp.sum(earlier * onehot, axis=1)
    position = flat_ids * capacity + slot_index
    slot_table = (
        jnp.full((all_experts * capacity,), assigned, jnp.int32)
        .at[position]
        .set(jnp.arange(assigned, dtype=jnp.int32))
    )
    filled = slot_table < assigned
    picked = jnp.minimum(slot_table, assigned - 1)
    token_pick = picked // top_k
    layout = (sources, local_experts, capacity, width_local)
    zero_bf = jnp.zeros((), jnp.bfloat16)
    send_tokens = jnp.where(filled[:, None], tokens[token_pick], zero_bf).reshape(layout)
    send_cot = jnp.where(filled[:, None], cotangent[token_pick], zero_bf).reshape(layout)
    send_weight = jnp.where(filled, route_weight.reshape(-1)[picked], jnp.float32(0.0)).reshape(
        layout[:3]
    )
    arrived_tokens, arrived_cot = (
        lax.all_to_all(send_tokens, EP, split_axis=0, concat_axis=0, tiled=True),
        lax.all_to_all(send_cot, EP, split_axis=0, concat_axis=0, tiled=True),
    )
    arrived_weight = stepwise_exchange(send_weight, EP, (0, 1), 0, 0)
    gate_pre = saved_gate.astype(jnp.float32)
    up_pre = saved_up.astype(jnp.float32)
    sigmoid_gate = jax.nn.sigmoid(gate_pre)
    hidden = gate_pre * sigmoid_gate * up_pre
    hidden_bf = hidden.astype(jnp.bfloat16)
    partial_back = jnp.einsum(
        "secd,efd->secf", arrived_cot, down_weight, preferred_element_type=jnp.float32
    )
    expert_out = jnp.einsum(
        "secf,efd->secd", hidden_bf, down_weight, preferred_element_type=jnp.float32
    )
    score_part = jnp.sum(expert_out * arrived_cot.astype(jnp.float32), axis=3)
    back_grad = lax.psum(partial_back.astype(jnp.bfloat16), "tp").astype(jnp.float32)
    score_total = lax.psum(score_part, "tp")
    score_back = stepwise_exchange(score_total, EP, (0, 1), 0, 0)
    route_grad = score_back.reshape(-1)[position].reshape(tok_rows, top_k)
    weights = arrived_weight[..., None]
    grad_hidden = weights * back_grad
    grad_up_pre = (grad_hidden * gate_pre * sigmoid_gate).astype(jnp.bfloat16)
    grad_gate_pre = (
        grad_hidden * up_pre * sigmoid_gate * (1.0 + gate_pre * (1.0 - sigmoid_gate))
    ).astype(jnp.bfloat16)
    weighted = (weights * hidden).astype(jnp.bfloat16)
    gate_weight_grad = jnp.einsum(
        "secd,secf->edf", arrived_tokens, grad_gate_pre, preferred_element_type=jnp.float32
    ).astype(jnp.bfloat16)
    up_weight_grad = jnp.einsum(
        "secd,secf->edf", arrived_tokens, grad_up_pre, preferred_element_type=jnp.float32
    ).astype(jnp.bfloat16)
    down_weight_grad = jnp.einsum(
        "secf,secd->efd", weighted, arrived_cot, preferred_element_type=jnp.float32
    ).astype(jnp.bfloat16)
    slot_grad = (
        jnp.einsum("secf,edf->secd", grad_gate_pre, gate_weight, preferred_element_type=jnp.float32)
        + jnp.einsum("secf,edf->secd", grad_up_pre, up_weight, preferred_element_type=jnp.float32)
    ).astype(jnp.bfloat16)
    grad_back = lax.all_to_all(slot_grad, EP, split_axis=0, concat_axis=0, tiled=True)
    token_rows_back = grad_back.reshape(all_experts * capacity, width_local)[position]
    token_grad = jnp.sum(
        token_rows_back.astype(jnp.float32).reshape(tok_rows, top_k, width_local), axis=1
    ).astype(jnp.bfloat16)
    return (token_grad, route_grad, gate_weight_grad, up_weight_grad, down_weight_grad)


def solution(mesh):
    split = Mesh(mesh.devices.reshape(8, 4, mesh.shape["tp"]), ("ep_0", "ep_1", "tp"))
    return jax.shard_map(
        local,
        mesh=split,
        in_specs=(
            P(EP, "tp"),
            P(EP, "tp"),
            P(EP, None),
            P(EP, None),
            P(EP, "tp", None),
            P(EP, "tp", None),
            P(EP, None, "tp"),
            P(None, EP, None, None),
            P(None, EP, None, None),
        ),
        out_specs=(
            P(EP, "tp"),
            P(EP, None),
            P(EP, "tp", None),
            P(EP, "tp", None),
            P(EP, None, "tp"),
        ),
        check_vma=False,
    )
```

profile of v0, /device:TPU:1, one launch (start us, length us, event | category | flops | bytes accessed | tf_op | source)
XLA Modules:
  0.0 298.1 jit_solution(8396807054021667519)
XLA Ops:
  9.5 18.0 %reduce-window.6 = s32[64,8,128]{2,1,0:T(8,128)S(1)} reduce-window(s32[64,8,128]{2,1,0:T(8,128)S(1)} %fusion.45, s32[]{:T(128)} %constant.15.clone.1), window={size=1x1x128 pad=0_0x0_0x127_0}, to_apply=%region_0.0 | reduce-window | flops 8323072 | bytes 524292 | tf_op jit(solution)/shard_map/reduce-window
  28.1 4.3 %scatter_custom_fusion = s32[2048]{0:T(1024)S(1)} fusion(s32[1024]{0:T(1024)S(1)} %bitcast.99, s32[1024]{0:T(1024)S(1)} %iota.11, s32[]{:T(128)} %constant.12.clone.1), kind=kCustom, calls=%fused_computation.73 | custom fusion | bytes 8196 | tf_op jit(solution)/shard_map/scatter | solution.py:62
  32.8 8.6 %gather_fusion = f32[2048]{0:T(1024)S(1)} fusion(f32[1024]{0:T(1024)S(1)} %reshape.83, s32[2048]{0:T(1024)S(1)} %get-tuple-element.26), kind=kCustom, calls=%fused_computation | custom fusion | bytes 24576 | tf_op jit(solution)/shard_map/gather | solution.py:71
  42.3 10.9 %all-to-all-start = ((f32[8,1,256]{2,1,0:T(1,128)}), f32[8,1,256]{2,1,0:T(1,128)S(1)}, u32[]{:S(2)}, u32[]{:S(2)}) async-start(f32[8,1,256]{2,1,0:T(1,128)} %reshape.145), calls=%async_computation | async-start | bytes 16384 | tf_op jit(solution)/shard_map/all_to_all | solution.py:25
  53.2 7.5 %gather_fusion.4 = bf16[2048,256]{1,0:T(8,128)(2,1)S(1)} fusion(bf16[512,256]{1,0:T(8,128)(2,1)S(1)} %copy-done.1, s32[2048]{0:T(1024)S(1)} %get-tuple-element.27), kind=kCustom, calls=%fused_computation.4 | custom fusion | bytes 2105344 | tf_op jit(solution)/shard_map/gather | solution.py:69
  60.7 7.5 %gather_fusion.1 = bf16[2048,256]{1,0:T(8,128)(2,1)S(1)} fusion(bf16[512,256]{1,0:T(8,128)(2,1)S(1)} %copy-done.2, s32[2048]{0:T(1024)S(1)} %get-tuple-element.27), kind=kCustom, calls=%fused_computation.1 | custom fusion | bytes 2105344 | tf_op jit(solution)/shard_map/gather | solution.py:70
  69.8 9.5 %all-to-all-start.2 = ((bf16[32,2,32,256]{3,2,1,0:T(8,128)(2,1)}), bf16[32,2,32,256]{3,2,1,0:T(8,128)(2,1)S(1)}, u32[]{:S(2)}, u32[]{:S(2)}) async-start(bf16[32,2,32,256]{3,2,1,0:T(8,128)(2,1)} %get-tuple-element.25), calls=%async_computation.2 | async-start | bytes 2097152 | tf_op jit(solution)/shard_map/all_to_all | solution.py:76
  81.3 23.9 %all-to-all-done.2 = bf16[32,2,32,256]{3,2,1,0:T(8,128)(2,1)S(1)} async-done(((bf16[32,2,32,256]{3,2,1,0:T(8,128)(2,1)}), bf16[32,2,32,256]{3,2,1,0:T(8,128)(2,1)S(1)}, u32[]{:S(2)}, u32[]{:S(2)}) %all-to-all-start.2) | async-done | bytes 1048608 | tf_op jit(solution)/shard_map/all_to_all | solution.py:76
  105.2 4.4 %all-to-all-start.1 = ((f32[4,1,512]{2,1,0:T(1,128)}), f32[4,1,512]{2,1,0:T(1,128)S(1)}, u32[]{:S(2)}, u32[]{:S(2)}) async-start(f32[4,1,512]{2,1,0:T(1,128)} %reshape.147), calls=%async_computation.1 | async-start | bytes 16384 | tf_op jit(solution)/shard_map/all_to_all | solution.py:25
  111.6 3.8 %fusion.10 = f32[32,2,32]{2,0,1:T(8,128)S(1)} fusion(bf16[32,2,32,256]{3,2,1,0:T(8,128)(2,1)S(1)} %all-to-all-done.2, bf16[2,512,256]{2,1,0:T(8,128)(2,1)S(1)} %copy-done, bf16[32,2,32,512]{3,2,1,0:T(8,128)(2,1)} %param.17, bf16[32,2,32,512]{3,2,1,0:T(8,128)(2,1)} %param.16), kind=kOutput, calls=%fused_computation.25 | convolution fusion | flops 546830336 | bytes 5775360 | tf_op jit(solution)/shard_map/secf,efd->secd/dot_general | solution.py:87
  115.5 46.0 %psum.15 = f32[8,4,1,2,32]{4,3,1,2,0:T(2,128)S(1)} all-reduce(f32[8,4,1,2,32]{4,3,1,2,0:T(2,128)S(1)} %copy.75), channel_id=1, replica_groups=mesh['ep_0'=8,'ep_1'=4,'tp'=16] {'tp'}, use_global_device_ids=true, to_apply=%region_7.8 | all-reduce | flops 2048 | bytes 16384 | tf_op jit(solution)/shard_map/psum | solution.py:92
  161.6 9.2 %all_to_all.35 = f32[8,1,256]{2,1,0:T(1,128)S(1)} all-to-all(f32[8,1,256]{2,1,0:T(1,128)S(1)} %reshape.149), channel_id=1, replica_groups=mesh['ep_0'=8,'ep_1'=4,'tp'=16] {'ep_0'}, dimensions={0} | all-to-all | bytes 16384 | tf_op jit(solution)/shard_map/all_to_all | solution.py:25
  170.8 5.3 %all-to-all-start.6 = ((bf16[32,2,32,256]{3,2,1,0:T(8,128)(2,1)}), bf16[32,2,32,256]{3,2,1,0:T(8,128)(2,1)}, u32[]{:S(2)}, u32[]{:S(2)}) async-start(bf16[32,2,32,256]{3,2,1,0:T(8,128)(2,1)} %get-tuple-element.24), calls=%async_computation.6 | async-start | bytes 2097152 | tf_op jit(solution)/shard_map/all_to_all | solution.py:75
  178.4 55.9 %all-reduce.2.cloned.1.call-done = bf16[32,2,32,512]{3,2,0,1:T(8,128)(2,1)} async-done(((bf16[32,2,32,512]{3,2,0,1:T(8,128)(2,1)}), bf16[32,2,32,512]{3,2,0,1:T(8,128)(2,1)}) %all-reduce.2.cloned.1.call-update) | async-done | bytes 2097168 | tf_op jit(solution)/shard_map/psum | solution.py:91
  234.3 4.3 %fusion.8 = (bf16[32,2,32,512]{3,2,0,1:T(8,128)(2,1)S(1)}, bf16[32,2,32,512]{3,2,0,1:T(8,128)(2,1)S(1)}) fusion(bf16[32,2,32,512]{3,2,0,1:T(8,128)(2,1)} %all-reduce.2.cloned.1.call-done, f32[32,2,32]{2,0,1:T(8,128)S(1)} %bitcast.91, bf16[32,2,32,512]{3,2,1,0:T(8,128)(2,1)} %param.16, bf16[32,2,32,512]{3,2,1,0:T(8,128)(2,1)} %param.17), kind=kLoop, calls=%fused_computation.20 | loop fusion | flops 17825792 | bytes 10493952 | tf_op jit(solution)/shard_map/convert_element_type | solution.py:97
  242.1 3.7 %all-to-all-start.5 = ((f32[4,1,512]{2,1,0:T(1,128)}), f32[4,1,512]{2,1,0:T(1,128)S(1)}, u32[]{:S(2)}, u32[]{:S(2)}) async-start(f32[4,1,512]{2,1,0:T(1,128)} %reshape.151), calls=%async_computation.5 | async-start | bytes 16384 | tf_op jit(solution)/shard_map/all_to_all | solution.py:25
  245.8 2.3 fusion.19
  250.0 9.5 %all-to-all-start.3 = ((bf16[32,2,32,256]{3,2,1,0:T(8,128)(2,1)}), bf16[32,2,32,256]{3,2,1,0:T(8,128)(2,1)S(1)}, u32[]{:S(2)}, u32[]{:S(2)}) async-start(bf16[32,2,32,256]{3,2,1,0:T(8,128)(2,1)} %copy.73), calls=%async_computation.3 | async-start | bytes 2097152 | tf_op jit(solution)/shard_map/all_to_all | solution.py:115
  259.6 4.7 %fusion.32 = bf16[2,512,256]{2,1,0:T(8,128)(2,1)} fusion(f32[32,2,32]{2,0,1:T(8,128)S(1)} %bitcast.92, bf16[32,2,32,256]{3,2,1,0:T(8,128)(2,1)S(1)} %copy-done.7, bf16[32,2,32,512]{3,2,1,0:T(8,128)(2,1)} %param.17, bf16[32,2,32,512]{3,2,1,0:T(8,128)(2,1)} %param.16), kind=kOutput, calls=%fused_computation.41 | convolution fusion | flops 546570240 | bytes 5775360 | tf_op jit(solution)/shard_map/secf,secd->efd/dot_general | solution.py:108
  265.1 6.1 %gather_fusion.3 = f32[1024]{0:T(1024)S(1)} fusion(f32[2048]{0:T(1024)S(1)} %reshape_reshape_reshape.7, s32[1024]{0:T(1024)S(1)} %broadcast_clamp_fusion), kind=kCustom, calls=%fused_computation.3 | custom fusion | bytes 12288 | tf_op jit(solution)/shard_map/gather | solution.py:94
  272.2 3.6 %fusion.26 = bf16[2,256,512]{2,1,0:T(8,128)(2,1)} fusion(bf16[32,2,32,256]{3,2,1,0:T(8,128)(2,1)} %all-to-all-done.6, bf16[32,2,32,512]{3,2,0,1:T(8,128)(2,1)} %copy-done.5), kind=kOutput, calls=%fused_computation.39 | convolution fusion | flops 537133056 | bytes 3670016 | tf_op jit(solution)/shard_map/secd,secf->edf/dot_general | solution.py:105
  275.8 2.8 fusion.29
  278.6 6.5 %all-to-all-done.3 = bf16[32,2,32,256]{3,2,1,0:T(8,128)(2,1)S(1)} async-done(((bf16[32,2,32,256]{3,2,1,0:T(8,128)(2,1)}), bf16[32,2,32,256]{3,2,1,0:T(8,128)(2,1)S(1)}, u32[]{:S(2)}, u32[]{:S(2)}) %all-to-all-start.3) | async-done | bytes 1048608 | tf_op jit(solution)/shard_map/all_to_all | solution.py:115
  285.1 3.9 %gather_fusion.2 = bf16[1024,256]{1,0:T(8,128)(2,1)S(1)} fusion(bf16[2048,256]{1,0:T(8,128)(2,1)S(1)} %bitcast.87, s32[1024]{0:T(1024)S(1)} %broadcast_clamp_fusion), kind=kCustom, calls=%fused_computation.2 | custom fusion | bytes 1052672 | tf_op jit(solution)/shard_map/gather | solution.py:116
  (79 shorter events, 21.3 us)
Async XLA Ops:
  7.2 102.4 %copy-start = (bf16[2,512,256]{2,1,0:T(8,128)(2,1)S(1)}, bf16[2,512,256]{2,1,0:T(8,128)(2,1)}, u32[]{:S(2)}) copy-start(bf16[2,512,256]{2,1,0:T(8,128)(2,1)} %param.15) | copy-start | bytes 1572868
  7.2 25.3 %copy-start.10 = (f32[512,2]{0,1:T(2,128)S(1)}, f32[512,2]{0,1:T(2,128)}, u32[]{:S(2)}) copy-start(f32[512,2]{0,1:T(2,128)} %param.12) | copy-start | bytes 12292
  32.8 20.4 %copy-start.1 = (bf16[512,256]{1,0:T(8,128)(2,1)S(1)}, bf16[512,256]{1,0:T(8,128)(2,1)}, u32[]{:S(2)}) copy-start(bf16[512,256]{1,0:T(8,128)(2,1)} %param.9) | copy-start | bytes 786436
  42.3 27.5 %all-to-all-start = ((f32[8,1,256]{2,1,0:T(1,128)}), f32[8,1,256]{2,1,0:T(1,128)S(1)}, u32[]{:S(2)}, u32[]{:S(2)}) async-start(f32[8,1,256]{2,1,0:T(1,128)} %reshape.145), calls=%async_computation | async-start | bytes 16384 | tf_op jit(solution)/shard_map/all_to_all | solution.py:25
  53.2 7.5 %copy-start.2 = (bf16[512,256]{1,0:T(8,128)(2,1)S(1)}, bf16[512,256]{1,0:T(8,128)(2,1)}, u32[]{:S(2)}) copy-start(bf16[512,256]{1,0:T(8,128)(2,1)} %param.10) | copy-start | bytes 786436
  69.8 35.4 %all-to-all-start.2 = ((bf16[32,2,32,256]{3,2,1,0:T(8,128)(2,1)}), bf16[32,2,32,256]{3,2,1,0:T(8,128)(2,1)S(1)}, u32[]{:S(2)}, u32[]{:S(2)}) async-start(bf16[32,2,32,256]{3,2,1,0:T(8,128)(2,1)} %get-tuple-element.25), calls=%async_computation.2 | async-start | bytes 2097152 | tf_op jit(solution)/shard_map/all_to_all | solution.py:76
  105.2 6.5 %copy-start.6 = (bf16[32,2,32,256]{3,2,1,0:T(8,128)(2,1)}, bf16[32,2,32,256]{3,2,1,0:T(8,128)(2,1)S(1)}, u32[]{:S(2)}) copy-start(bf16[32,2,32,256]{3,2,1,0:T(8,128)(2,1)S(1)} %all-to-all-done.2) | copy-start | bytes 3145732
  105.2 56.5 %all-to-all-start.1 = ((f32[4,1,512]{2,1,0:T(1,128)}), f32[4,1,512]{2,1,0:T(1,128)S(1)}, u32[]{:S(2)}, u32[]{:S(2)}) async-start(f32[4,1,512]{2,1,0:T(1,128)} %reshape.147), calls=%async_computation.1 | async-start | bytes 16384 | tf_op jit(solution)/shard_map/all_to_all | solution.py:25
  109.5 124.8 %all-reduce.2.cloned.1.call-start = ((), (), s32[]{:S(2)}) async-start(), calls=%async_computation.7 | async-start | bytes 4194304 | tf_op jit(solution)/shard_map/psum | solution.py:91
  170.8 71.3 %all-to-all-start.6 = ((bf16[32,2,32,256]{3,2,1,0:T(8,128)(2,1)}), bf16[32,2,32,256]{3,2,1,0:T(8,128)(2,1)}, u32[]{:S(2)}, u32[]{:S(2)}) async-start(bf16[32,2,32,256]{3,2,1,0:T(8,128)(2,1)} %get-tuple-element.24), calls=%async_computation.6 | async-start | bytes 2097152 | tf_op jit(solution)/shard_map/all_to_all | solution.py:75
  234.3 5.7 %copy-start.8 = (bf16[2,256,512]{2,1,0:T(8,128)(2,1)S(1)}, bf16[2,256,512]{2,1,0:T(8,128)(2,1)}, u32[]{:S(2)}) copy-start(bf16[2,256,512]{2,1,0:T(8,128)(2,1)} %param.13) | copy-start | bytes 1572868
  238.7 1.4 copy-start.3
  238.7 7.1 %copy-start.5 = (bf16[32,2,32,512]{3,2,0,1:T(8,128)(2,1)}, bf16[32,2,32,512]{3,2,0,1:T(8,128)(2,1)S(1)}, u32[]{:S(2)}) copy-start(bf16[32,2,32,512]{3,2,0,1:T(8,128)(2,1)S(1)} %get-tuple-element.22) | copy-start | bytes 6291460
  240.0 5.8 %copy-start.9 = (bf16[2,256,512]{2,1,0:T(8,128)(2,1)S(1)}, bf16[2,256,512]{2,1,0:T(8,128)(2,1)}, u32[]{:S(2)}) copy-start(bf16[2,256,512]{2,1,0:T(8,128)(2,1)} %param.14) | copy-start | bytes 1572868
  242.1 7.9 %all-to-all-start.5 = ((f32[4,1,512]{2,1,0:T(1,128)}), f32[4,1,512]{2,1,0:T(1,128)S(1)}, u32[]{:S(2)}, u32[]{:S(2)}) async-start(f32[4,1,512]{2,1,0:T(1,128)} %reshape.151), calls=%async_computation.5 | async-start | bytes 16384 | tf_op jit(solution)/shard_map/all_to_all | solution.py:25
  248.2 11.4 %copy-start.7 = (bf16[32,2,32,256]{3,2,1,0:T(8,128)(2,1)S(1)}, bf16[32,2,32,256]{3,2,1,0:T(8,128)(2,1)}, u32[]{:S(2)}) copy-start(bf16[32,2,32,256]{3,2,1,0:T(8,128)(2,1)} %copy-done.6) | copy-start | bytes 3145732
  250.0 35.1 %all-to-all-start.3 = ((bf16[32,2,32,256]{3,2,1,0:T(8,128)(2,1)}), bf16[32,2,32,256]{3,2,1,0:T(8,128)(2,1)S(1)}, u32[]{:S(2)}, u32[]{:S(2)}) async-start(bf16[32,2,32,256]{3,2,1,0:T(8,128)(2,1)} %copy.73), calls=%async_computation.3 | async-start | bytes 2097152 | tf_op jit(solution)/shard_map/all_to_all | solution.py:115
  272.2 3.6 %copy-start.4 = (bf16[32,2,32,512]{3,2,0,1:T(8,128)(2,1)S(1)}, bf16[32,2,32,512]{3,2,0,1:T(8,128)(2,1)}, u32[]{:S(2)}) copy-start(bf16[32,2,32,512]{3,2,0,1:T(8,128)(2,1)} %copy-done.3) | copy-start | bytes 6291460
Sparse Core Ops, SparseCore 0:
  112.7 121.5 all-reduce.1
where the time goes:
time: 302 us; the launch traced here: 298 us
  waiting for transfers between devices  87.1 us (29%)
  blocking collectives  55.2 us (18%)
  local copies, waits for them, and re-layouts  47.1 us (16%)
  starting transfers between devices  43.3 us (14%)
  other arithmetic  29.7 us (10%)
  matrix products  21.3 us (7%)
  between operations  14.4 us (5%)
    psum x1, waiting for transfers between devices, local(): lax.psum(partial_back.astype(jnp.bfloat16), 'tp').astype(jnp.float32)  55.9 us
    psum x1, blocking collectives, local(): score_total = lax.psum(score_part, 'tp')  46 us
    all_to_all x1, waiting for transfers between devices, local(): lax.all_to_all(send_cot, EP, split_axis=0, concat_axis=0, tiled=True)  23.9 us
    all_to_all x3, starting transfers between devices, moved_by_axis(): lax.all_to_all(tiles, axes[k], split_axis=k, concat_axis=k, tiled=True)  19 us
    another operation x3, other arithmetic  18.2 us
    all_to_all x1, starting transfers between devices, local(): lax.all_to_all(slot_grad, EP, split_axis=0, concat_axis=0, tiled=True)  9.53 us
    all_to_all x1, starting transfers between devices, local(): lax.all_to_all(send_cot, EP, split_axis=0, concat_axis=0, tiled=True)  9.5 us
    all_to_all x1, blocking collectives, moved_by_axis(): lax.all_to_all(tiles, axes[k], split_axis=k, concat_axis=k, tiled=True)  9.2 us
  transfers between devices with their start and end apart: 7, of which 4 were waited for; matrix products, arithmetic and copies ran while one was open for 19% of the time, Pallas kernels for 0%

commit v1 on v0

v1 whole, which is shorter than its diff:
```python
import functools

import jax
import jax.numpy as jnp
from jax import lax
from jax.experimental import pallas as pl
from jax.experimental.pallas import tpu as pltpu
from jax.sharding import Mesh
from jax.sharding import PartitionSpec as P

EP = ("z", "x")
TP = ("y", "c")
NX = 4
CAP = 32
SEATS = 64
ROWS = NX * CAP
F32 = jnp.float32
BF16 = jnp.bfloat16
DY, XT, META = 0, 1, 2


def dot(a, b, ca=1, cb=0):
    return lax.dot_general(a, b, (((ca,), (cb,)), ((), ())), preferred_element_type=F32)


def kernel(
    nz, ids_ref, rw_ref, tok_ref, cot_ref, gate_hbm, up_hbm, down_hbm, sg_hbm, su_hbm,
    tg_ref, rg_ref, gg_ref, ug_ref, dg_ref,
    gate, up, down, sg, su, pre_u, pre_g, hid, pw, gmat,
    sz, szm, rz, rzm, rx, rxm, perm, wcol, slots,
    zp, zr, rss, rsr, zf, du, dg, ts, tsm, cx, cxm, bs, bsm, br, brm,
    lsem, zss, zrs, xss, xrs, pss, prs, rcs, rcr, acs, acr, qss, qrs, vss, vrs, wss, wrs,
):
    zi, xi, yi, ci = (lax.axis_index(a) for a in ("z", "x", "y", "c"))
    ny = nz
    hf = zf.shape[-1]
    tokens = tok_ref.shape[0]
    left_half = lax.div(xi, 2) == 0
    my_row = 2 * lax.rem(xi, 2)
    seat0 = pl.multiple_of(SEATS * lax.div(xi, 2), SEATS)

    def far_first(k):
        k2 = nz - k
        return jnp.where(lax.rem(k2, 2) == 1, lax.div(k2 + 1, 2), nz - lax.div(k2, 2))

    def remote(src, dst, ssem, rsem, **where):
        return pltpu.make_async_remote_copy(
            src_ref=src, dst_ref=dst, send_sem=ssem, recv_sem=rsem,
            device_id=where, device_id_type=pl.DeviceIdType.MESH,
        )

    loads = [
        pltpu.make_async_copy(src, dst, lsem.at[i])
        for i, (src, dst) in enumerate(
            ((sg_hbm, sg), (su_hbm, su), (down_hbm, down), (gate_hbm, gate), (up_hbm, up))
        )
    ]
    for copy in loads:
        copy.start()

    barrier = pltpu.get_barrier_semaphore()

    def greet(**where):
        pl.semaphore_signal(barrier, 1, device_id=where, device_id_type=pl.DeviceIdType.MESH)

    for k in range(1, nz):
        greet(z=lax.rem(zi + k, nz))
    for k in range(1, NX):
        greet(x=lax.rem(xi + k, NX))
    greet(y=lax.rem(yi + 1, ny))
    greet(y=lax.rem(yi + ny - 1, ny))
    greet(c=1 - ci)

    experts, groups = 4 * 2 * nz, 2 * nz
    id0, id1 = ids_ref[0:1, :], ids_ref[1:2, :]
    rw0, rw1 = rw_ref[0:1, :], rw_ref[1:2, :]
    group = lax.shift_right_logical(id0, 2)
    erow = lax.broadcasted_iota(jnp.int32, (experts, tokens), 0)
    hot0, hot1 = erow == id0, erow == id1
    chosen = jnp.where(hot0, 1.0, 0.0) + jnp.where(hot1, 1.0, 0.0)
    grow = lax.broadcasted_iota(jnp.int32, (groups, tokens), 0)
    ingroup = jnp.where(grow == group, 1.0, 0.0)
    earlier = jnp.where(
        lax.broadcasted_iota(jnp.int32, (tokens, tokens), 0)
        < lax.broadcasted_iota(jnp.int32, (tokens, tokens), 1),
        1.0, 0.0,
    ).astype(BF16)
    count = dot(jnp.concatenate([chosen, ingroup], axis=0).astype(BF16), earlier)
    rank = jnp.sum(ingroup * count[experts:], axis=0, keepdims=True)
    target = group * SEATS + rank.astype(jnp.int32)
    weight = jnp.where(hot0, rw0, 0.0) + jnp.where(hot1, rw1, 0.0)
    weight_hi = weight.astype(BF16).astype(F32)
    pw[0] = chosen * (count[:experts] + 1.0)
    pw[1] = weight_hi
    pw[2] = weight - weight_hi

    def seat_rows(zt):
        row = lax.broadcasted_iota(jnp.int32, (2 * SEATS, tokens), 0) + zt * (2 * SEATS)
        return jnp.where(row == target, 1.0, 0.0).astype(BF16)

    def gathered(zt):
        g = seat_rows(zt)
        gmat[pl.ds(pl.multiple_of(zt * 2 * SEATS, 2 * SEATS), 2 * SEATS), :] = g
        e0 = pl.multiple_of(zt * 8, 8)
        lhs = jnp.concatenate([pw[i, pl.ds(e0, 8), :] for i in range(3)], axis=0).astype(BF16)
        r = dot(lhs, g, 1, 1)
        tile = jnp.concatenate(
            [r[0:4] + r[4:8], (r[8:12] + r[12:16]) + (r[16:20] + r[20:24])], axis=0
        )
        return dot(g, cot_ref[...]).astype(BF16), tile

    rows, tile = gathered(zi)
    rz[DY, zi] = rows
    rzm[zi] = tile
    pl.semaphore_wait(barrier, (nz - 1) + (NX - 1) + 3)

    def z_copy(which, zt, zs):
        if which == META:
            return remote(szm.at[zt], rzm.at[zs], zss.at[META, zt], zrs.at[META, zs], z=zt)
        return remote(sz.at[which, zt], rz.at[which, zs], zss.at[which, zt], zrs.at[which, zs], z=zt)

    def send_dy(k, _):
        zt = lax.rem(zi + far_first(k), nz)
        rows, tile = gathered(zt)
        szm[zt] = tile
        sz[DY, zt] = rows
        z_copy(META, zt, zi).start()
        z_copy(DY, zt, zi).start()
        return 0

    lax.fori_loop(1, nz, send_dy, 0)

    def rows_of_tokens(zt):
        g = gmat[pl.ds(pl.multiple_of(zt * 2 * SEATS, 2 * SEATS), 2 * SEATS), :]
        return dot(g, tok_ref[...]).astype(BF16)

    def send_x(k, _):
        zt = lax.rem(zi + far_first(k), nz)
        sz[XT, zt] = rows_of_tokens(zt)
        z_copy(XT, zt, zi).start()
        return 0

    lax.fori_loop(1, nz, send_x, 0)
    rz[XT, zi] = rows_of_tokens(zi)

    loads[0].wait()
    loads[1].wait()

    def elementwise(i, _):
        q, j = lax.div(i, 2), lax.rem(i, 2)
        g = sg[pl.ds(NX * q, NX), j].astype(F32).reshape(ROWS, -1)
        u = su[pl.ds(NX * q, NX), j].astype(F32).reshape(ROWS, -1)
        s = jax.nn.sigmoid(g)
        gs = g * s
        pre_u[j, q] = gs
        pre_g[j, q] = u * s * (1.0 + g * (1.0 - s))
        hid[j, q] = gs * u
        return 0

    lax.fori_loop(0, 2 * nz, elementwise, 0)

    def came(k):
        return jnp.where(k == 0, zi, lax.rem(zi + nz - far_first(jnp.maximum(k, 1)), nz))

    def x_copy(which, q, xt, xs):
        if which == META:
            return remote(rzm.at[q], rxm.at[q, xs], xss.at[META, q, xt], xrs.at[META, q, xs], x=xt)
        seats = pl.ds(pl.multiple_of(SEATS * lax.div(xt, 2), SEATS), SEATS)
        return remote(
            rz.at[which, q, seats], rx.at[which, q, xs],
            xss.at[which, q, xt], xrs.at[which, q, xs], x=xt,
        )

    def spread(which, q):
        for d in range(1, NX):
            x_copy(which, q, lax.rem(xi + d, NX), xi).start()

    def pass_dy(q):
        spread(META, q)
        spread(DY, q)
        rx[DY, q, xi] = rz[DY, q, pl.ds(seat0, SEATS), :]
        rxm[q, xi] = rzm[q]

    def take_dy(k):
        q = came(k)
        z_copy(META, q, q).wait_recv()
        z_copy(DY, q, q).wait_recv()
        pass_dy(q)

    loads[2].wait()

    def pair_copy(q):
        return remote(zp.at[q, 1 - ci], zr.at[q], pss.at[q], prs.at[q], c=1 - ci)

    def back_partial(k):
        q = came(k)
        for d in range(1, NX):
            xs = lax.rem(xi + d, NX)
            x_copy(META, q, xs, xs).wait_recv()
            x_copy(DY, q, xs, xs).wait_recv()
        t = rxm[q]
        t = jnp.where(left_half, t[:, :, :SEATS], t[:, :, SEATS:])
        line = lax.broadcasted_iota(jnp.int32, t.shape, 1)

        def lanes(i):
            v = jnp.sum(jnp.where(line == i, t, 0.0), axis=1)
            return jnp.concatenate([v[n : n + 1] for n in range(NX)], axis=1)

        base = CAP * lax.div(lax.broadcasted_iota(jnp.int32, (1, NX * SEATS), 1), SEATS)
        slot = lax.broadcasted_iota(jnp.int32, (ROWS, NX * SEATS), 0)
        for j in range(2):
            place = lanes(my_row + j).astype(jnp.int32)
            key = jnp.where(place > 0, place - 1 + base, -1)
            hit = slot == key
            perm[q, pl.ds(j * ROWS, ROWS), :] = jnp.where(hit, 1.0, 0.0).astype(BF16)
            w = jnp.sum(jnp.where(hit, lanes(4 + my_row + j), 0.0), axis=1, keepdims=True)
            wcol[j, q] = jnp.broadcast_to(w, (ROWS, 128))
        arrived = rx[DY, q].reshape(NX * SEATS, -1)
        moved = dot(perm[q], arrived).astype(BF16)
        for j in range(2):
            part = moved[j * ROWS : (j + 1) * ROWS]
            slots[DY, j, q] = part
            z = dot(part, down[j], 1, 1).astype(BF16)
            zp[q, 0, j] = z[:, :hf]
            zp[q, 1, j] = z[:, hf:]
        pair_copy(q).start()

    pass_dy(zi)
    lag = 2 if nz > 2 else 1
    for k in range(1, lag):
        take_dy(jnp.int32(k))

    def steady(k, _):
        take_dy(k)
        back_partial(k - lag)
        return 0

    lax.fori_loop(lag, nz, steady, 0)

    def rest(k, _):
        back_partial(k)
        return 0

    lax.fori_loop(nz - lag, nz, rest, 0)

    def wait_pair(q, _):
        pair_copy(q).wait_recv()
        return 0

    lax.fori_loop(0, nz, wait_pair, 0)

    hops = {(0, 0): ny // 2, (0, 1): ny - 1 - ny // 2, (1, 0): ny - 1 - ny // 2, (1, 1): ny // 2}
    flows = [f for f in hops]

    def at_y(d):
        return lax.rem(yi + d + 2 * ny, ny)

    def own(q, j):
        return zp[q, ci, j].astype(F32) + zr[q, j].astype(F32)

    def rs_copy(j, way, s):
        step = 1 - 2 * way
        return remote(
            rss.at[j, way, s - 1], rsr.at[j, way, s - 1],
            rcs.at[j, way, s - 1], rcr.at[j, way, s - 1], y=at_y(step),
        )

    for s in range(1, ny // 2 + 1):
        for j, way in flows:
            if s > hops[j, way]:
                continue
            total = own(at_y((1 - 2 * way) * (hops[j, way] + 1 - s)), j)
            if s > 1:
                rs_copy(j, way, s - 1).wait_recv()
                total = total + rsr[j, way, s - 2].astype(F32)
            rss[j, way, s - 1] = total.astype(BF16)
            rs_copy(j, way, s).start()
        if s == 1:
            def down_grads(j, _):
                def weigh(q, _):
                    w = jnp.concatenate([wcol[j, q]] * (hid.shape[-1] // 128), axis=1)
                    du[j, q] = (w * hid[j, q]).astype(BF16)
                    return 0

                lax.fori_loop(0, nz, weigh, 0)
                hw = du[j].reshape(nz * ROWS, -1)
                dy = slots[DY, j].reshape(nz * ROWS, -1)
                dg_ref[j] = dot(hw, dy, 0, 0).astype(BF16)
                return 0

            lax.fori_loop(0, 2, down_grads, 0)

    for j in range(2):
        total = own(yi, j)
        for way in range(2):
            if hops[j, way] > 0:
                rs_copy(j, way, hops[j, way]).wait_recv()
                total = total + rsr[j, way, hops[j, way] - 1].astype(F32)
        zf[yi, ci, j] = total.astype(BF16)

    def ag_copy(j, way, s):
        step = 1 - 2 * way
        q = at_y(-step * (s - 1))
        return remote(
            zf.at[q, ci, j], zf.at[q, ci, j],
            acs.at[j, way, s - 1], acr.at[j, way, s - 1], y=at_y(step),
        )

    def ag_wait(j, way, s):
        q = at_y(-(1 - 2 * way) * s)
        remote(
            zf.at[q, ci, j], zf.at[q, ci, j],
            acs.at[j, way, s - 1], acr.at[j, way, s - 1], y=yi,
        ).wait_recv()
        return q

    def half_copy(q, j, h):
        return remote(zf.at[q, h, j], zf.at[q, h, j], qss.at[q, j], qrs.at[q, j], c=1 - ci)

    for j, way in flows:
        if hops[j, way] > 0:
            ag_copy(j, way, 1).start()
    for j in range(2):
        half_copy(yi, j, ci).start()

    def take_x(q, _):
        @pl.when(q != zi)
        def _():
            z_copy(XT, q, q).wait_recv()

        spread(XT, q)
        rx[XT, q, xi] = rz[XT, q, pl.ds(seat0, SEATS), :]
        return 0

    lax.fori_loop(0, nz, take_x, 0)
    loads[3].wait()
    loads[4].wait()

    def back_copy(q, xt, xs):
        return remote(ts.at[q, xt], cx.at[q, xs], vss.at[0, q, xt], vrs.at[0, q, xs], x=xt)

    def back_meta(q, xt, xs):
        return remote(tsm.at[q, xt], cxm.at[q, xs], vss.at[1, q, xt], vrs.at[1, q, xs], x=xt)

    def consume(q):
        for j in range(2):
            half_copy(q, j, 1 - ci).wait_recv()
        grads, tiles = [], None
        line = lax.broadcasted_iota(jnp.int32, (8, 2 * SEATS), 0)
        side = lax.div(lax.broadcasted_iota(jnp.int32, (8, 2 * SEATS), 1), SEATS) == lax.div(xi, 2)
        for j in range(2):
            z = jnp.concatenate([zf[q, 0, j], zf[q, 1, j]], axis=1).astype(F32)
            w = jnp.concatenate([wcol[j, q]] * (z.shape[-1] // 128), axis=1)
            wz = w * z
            up_grad = (wz * pre_u[j, q]).astype(BF16)
            gate_grad = (wz * pre_g[j, q]).astype(BF16)
            du[j, q] = up_grad
            dg[j, q] = gate_grad
            hb = hid[j, q].astype(BF16).astype(F32)
            score = jnp.sum(hb * z, axis=1, keepdims=True)
            p = perm[q, pl.ds(j * ROWS, ROWS), :].astype(F32)
            seat_score = jnp.sum(p * score, axis=0, keepdims=True)
            s = dot(gate_grad, gate[j], 1, 1) + dot(up_grad, up[j], 1, 1)
            grads.append(s.astype(BF16))
            mask = side & (line == my_row + j)
            made = []
            for n in range(NX):
                one = seat_score[:, n * SEATS : (n + 1) * SEATS]
                made.append(jnp.where(mask, jnp.concatenate([one, one], axis=1), 0.0))
            tiles = made if tiles is None else [a + b for a, b in zip(tiles, made)]
        for n in range(NX):
            tsm[q, n] = tiles[n]
        t = dot(perm[q], jnp.concatenate(grads, axis=0), 0, 0).astype(BF16)
        ts[q] = t.reshape(NX, SEATS, -1)
        for d in range(1, NX):
            xt = lax.rem(xi + d, NX)
            back_meta(q, xt, xi).start()
            back_copy(q, xt, xi).start()
        cx[q, xi] = ts[q, xi]
        cxm[q, xi] = tsm[q, xi]

    def home_copy(q, zs):
        return remote(bs.at[q], br.at[zs], wss.at[0, q], wrs.at[0, zs], z=q)

    def home_meta(q, zs):
        return remote(bsm.at[q], brm.at[zs], wss.at[1, q], wrs.at[1, zs], z=q)

    def combine(q):
        for d in range(1, NX):
            xs = lax.rem(xi + d, NX)
            back_meta(q, xs, xs).wait_recv()
            back_copy(q, xs, xs).wait_recv()
        first = (cx[q, 0].astype(F32) + cx[q, 1].astype(F32)).astype(BF16)
        second = (cx[q, 2].astype(F32) + cx[q, 3].astype(F32)).astype(BF16)
        scores = (cxm[q, 0] + cxm[q, 1]) + (cxm[q, 2] + cxm[q, 3])

        @pl.when(q == zi)
        def _():
            br[q, pl.ds(0, SEATS), :] = first
            br[q, pl.ds(SEATS, SEATS), :] = second
            brm[q] = scores

        @pl.when(q != zi)
        def _():
            bs[q, pl.ds(0, SEATS), :] = first
            bs[q, pl.ds(SEATS, SEATS), :] = second
            bsm[q] = scores
            home_meta(q, zi).start()
            home_copy(q, zi).start()

    half = ny // 2

    def order(i):
        d = lax.div(i + 1, 2)
        return at_y(jnp.where(lax.rem(i, 2) == 1, -d, d))

    done = 0
    mixed = 0
    for s in range(1, half + 2):
        if s <= half:
            for j, way in flows:
                if s > hops[j, way]:
                    continue
                q = ag_wait(j, way, s)
                if s + 1 <= hops[j, way]:
                    ag_copy(j, way, s + 1).start()
                half_copy(q, j, ci).start()
        upto = 1 if s == 1 else min(2 * s - 1, ny) if s <= half else ny

        def step(i, _):
            consume(order(i))
            return 0

        lax.fori_loop(done, upto, step, 0)
        done = upto
        ready = max(0, upto - 3) if s <= half else ny

        def join(i, _):
            combine(order(i))
            return 0

        lax.fori_loop(mixed, ready, join, 0)
        mixed = ready

    def seat_x(q, _):
        for d in range(1, NX):
            xs = lax.rem(xi + d, NX)
            x_copy(XT, q, xs, xs).wait_recv()
        moved = dot(perm[q], rx[XT, q].reshape(NX * SEATS, -1)).astype(BF16)
        slots[XT, 0, q] = moved[:ROWS]
        slots[XT, 1, q] = moved[ROWS:]
        return 0

    lax.fori_loop(0, nz, seat_x, 0)

    def weight_grads(j, _):
        x = slots[XT, j].reshape(nz * ROWS, -1)
        gg_ref[j] = dot(x, dg[j].reshape(nz * ROWS, -1), 0, 0).astype(BF16)
        ug_ref[j] = dot(x, du[j].reshape(nz * ROWS, -1), 0, 0).astype(BF16)
        return 0

    lax.fori_loop(0, 2, weight_grads, 0)

    def wait_home(k, _):
        q = lax.rem(zi + k, nz)
        home_meta(q, q).wait_recv()
        home_copy(q, q).wait_recv()
        return 0

    lax.fori_loop(1, nz, wait_home, 0)
    tg_ref[...] = dot(gmat[...], br[...].reshape(nz * 2 * SEATS, -1), 0, 0).astype(BF16)
    scores = jnp.concatenate([brm[q] for q in range(nz)], axis=1)
    hi = scores.astype(BF16)
    rest1 = scores - hi.astype(F32)
    mid = rest1.astype(BF16)
    low = (rest1 - mid.astype(F32)).astype(BF16)
    g = gmat[...]
    picked = dot(hi, g) + dot(mid, g) + dot(low, g)
    line = lax.broadcasted_iota(jnp.int32, picked.shape, 0)
    rg_ref[0:1, :] = jnp.sum(jnp.where(line == (id0 & 3), picked, 0.0), axis=0, keepdims=True)
    rg_ref[1:2, :] = jnp.sum(jnp.where(line == (id1 & 3), picked, 0.0), axis=0, keepdims=True)

    def drain_z(k, _):
        zt = lax.rem(zi + k, nz)
        for which in (META, DY, XT):
            z_copy(which, zt, zi).wait_send()
        home_meta(zt, zi).wait_send()
        home_copy(zt, zi).wait_send()
        return 0

    lax.fori_loop(1, nz, drain_z, 0)

    def drain_q(q, _):
        for d in range(1, NX):
            xt = lax.rem(xi + d, NX)
            for which in (META, DY, XT):
                x_copy(which, q, xt, xi).wait_send()
            back_meta(q, xt, xi).wait_send()
            back_copy(q, xt, xi).wait_send()
        pair_copy(q).wait_send()
        for j in range(2):
            half_copy(q, j, ci).wait_send()
        return 0

    lax.fori_loop(0, nz, drain_q, 0)
    for j, way in flows:
        for s in range(1, hops[j, way] + 1):
            rs_copy(j, way, s).wait_send()
            ag_copy(j, way, s).wait_send()


def local(nz, ids, rw, tok, cot, gate, up, down, sg, su):
    tokens, wide = tok.shape
    f = gate.shape[-1]
    hf = f // 2
    ny = nz
    experts = 8 * nz
    vm = pltpu.VMEM
    dma = pltpu.SemaphoreType.DMA
    steps = max(ny // 2, 1)
    scratch = [
        vm(gate.shape, BF16), vm(up.shape, BF16), vm(down.shape, BF16),
        vm(sg.shape, BF16), vm(su.shape, BF16),
        vm((2, nz, ROWS, f), F32), vm((2, nz, ROWS, f), F32), vm((2, nz, ROWS, f), F32),
        vm((3, experts, tokens), F32), vm((nz * 2 * SEATS, tokens), BF16),
        vm((2, nz, 2 * SEATS, wide), BF16), vm((nz, 8, 128), F32),
        vm((2, nz, 2 * SEATS, wide), BF16), vm((nz, 8, 128), F32),
        vm((2, nz, NX, SEATS, wide), BF16), vm((nz, NX, 8, 128), F32),
        vm((nz, 2 * ROWS, NX * SEATS), BF16), vm((2, nz, ROWS, 128), F32),
        vm((2, 2, nz, ROWS, wide), BF16),
        vm((nz, 2, 2, ROWS, hf), BF16), vm((nz, 2, ROWS, hf), BF16),
        vm((2, 2, steps, ROWS, hf), BF16), vm((2, 2, steps, ROWS, hf), BF16),
        vm((nz, 2, 2, ROWS, hf), BF16),
        vm((2, nz, ROWS, f), BF16), vm((2, nz, ROWS, f), BF16),
        vm((nz, NX, SEATS, wide), BF16), vm((nz, NX, 8, 128), F32),
        vm((nz, NX, SEATS, wide), BF16), vm((nz, NX, 8, 128), F32),
        vm((nz, 2 * SEATS, wide), BF16), vm((nz, 8, 128), F32),
        vm((nz, 2 * SEATS, wide), BF16), vm((nz, 8, 128), F32),
        dma((5,)), dma((3, nz)), dma((3, nz)), dma((3, nz, NX)), dma((3, nz, NX)),
        dma((nz,)), dma((nz,)), dma((2, 2, steps)), dma((2, 2, steps)),
        dma((2, 2, steps)), dma((2, 2, steps)), dma((nz, 2)), dma((nz, 2)),
        dma((2, nz, NX)), dma((2, nz, NX)), dma((2, nz)), dma((2, nz)),
    ]
    inside = pl.BlockSpec(memory_space=pltpu.VMEM)
    outside = pl.BlockSpec(memory_space=pl.ANY)
    out = pl.pallas_call(
        functools.partial(kernel, nz),
        out_shape=(
            jax.ShapeDtypeStruct(tok.shape, BF16),
            jax.ShapeDtypeStruct((2, tokens), F32),
            jax.ShapeDtypeStruct(gate.shape, BF16),
            jax.ShapeDtypeStruct(up.shape, BF16),
            jax.ShapeDtypeStruct(down.shape, BF16),
        ),
        in_specs=[inside] * 4 + [outside] * 5,
        out_specs=(inside,) * 5,
        scratch_shapes=scratch,
        compiler_params=pltpu.CompilerParams(
            collective_id=0, has_side_effects=True, vmem_limit_bytes=60 * 1024 * 1024
        ),
    )(ids.T, rw.T, tok, cot, gate, up, down, sg, su)
    return (out[0], out[1].T, *out[2:])


def on_axes(mesh, nz):
    return jax.shard_map(
        functools.partial(
            lambda n, tok, cot, ids, rw, *others: local(n, ids, rw, tok, cot, *others), nz
        ),
        mesh=mesh,
        in_specs=(
            P(EP, TP), P(EP, TP), P(EP, None), P(EP, None),
            P(EP, TP, None), P(EP, TP, None), P(EP, None, TP),
            P(None, EP, None, None), P(None, EP, None, None),
        ),
        out_specs=(
            P(EP, TP), P(EP, None), P(EP, TP, None), P(EP, TP, None), P(EP, None, TP),
        ),
        check_vma=False,
    )


def solution(mesh):
    nz = mesh.shape["ep"] // NX
    return on_axes(Mesh(mesh.devices.reshape(nz, NX, nz, 2), ("z", "x", "y", "c")), nz)
```

time: 302 us -> 104 us (0.34)
  the two profiles are of different devices: /device:TPU:1 before, /device:TPU:16 now
where the time goes in v1:
time: 104 us
  Pallas kernels  95.9 us (92%)
  local copies, waits for them, and re-layouts  7.53 us (7%)
    pallas_call x1, Pallas kernels, local(): pl.pallas_call(functools.partial(kernel, nz), out_shape=(jax.ShapeDtypeSt...  95.9 us
    unnamed x7, local copies, waits for them, and re-layouts  7.53 us

profile of v1, /device:TPU:16, one launch (start us, length us, event | category | flops | bytes accessed | tf_op | source)
XLA Modules:
  0.0 104.0 jit_solution(11980567853119699967)
XLA Ops:
  0.6 95.9 %shard_map.128 = (bf16[512,256]{1,0:T(8,128)(2,1)}, f32[2,512]{1,0:T(2,128)}, bf16[2,256,512]{2,1,0:T(8,128)(2,1)}, bf16[2,256,512]{2,1,0:T(8,128)(2,1)}, bf16[2,512,256]{2,1,0:T(8,128)(2,1)}) custom-call(s32[2,512]{1,0:T(2,128)} %bitcast.3, f32[2,512]{1,0:T(2,128)} %bitcast.4, bf16[512,256]{1,0:T(8,128)(2,1)} %tok_ref.1, bf16[512,256]{1,0:T(8,128)(2,1)} %cot_ref.1, ...), custom_call_target="tpu_custom_call" | custom-call | tf_op jit(solution)/shard_map/pallas_call | solution.py:546
  96.5 0.0 copy-start
  96.5 1.7 %copy.19 = bf16[512,256]{1,0:T(8,128)(2,1)} copy(bf16[512,256]{1,0:T(8,128)(2,1)} %get-tuple-element.20) | data formatting | bytes 524288
  98.2 1.3 %copy.20 = f32[512,2]{0,1:T(2,128)} copy(f32[512,2]{0,1:T(2,128)} %bitcast.5) | data formatting | bytes 8192
  99.5 1.9 %copy.21 = bf16[2,256,512]{2,1,0:T(8,128)(2,1)} copy(bf16[2,256,512]{2,1,0:T(8,128)(2,1)} %get-tuple-element.22) | data formatting | bytes 1048576
  101.4 1.9 %copy.22 = bf16[2,256,512]{2,1,0:T(8,128)(2,1)} copy(bf16[2,256,512]{2,1,0:T(8,128)(2,1)} %get-tuple-element.23) | data formatting | bytes 1048576
  103.2 0.0 copy-done
  103.2 0.8 copy.23
Async XLA Ops:
  96.5 6.7 %copy-start = (bf16[2,512,256]{2,1,0:T(8,128)(2,1)S(1)}, bf16[2,512,256]{2,1,0:T(8,128)(2,1)}, u32[]{:S(2)}) copy-start(bf16[2,512,256]{2,1,0:T(8,128)(2,1)} %get-tuple-element.24) | copy-start | bytes 1572868

commit v2 on v1

v2 whole, which is shorter than its diff:
```python
import functools

import jax
import jax.numpy as jnp
from jax import lax
from jax.experimental import pallas as pl
from jax.experimental.pallas import tpu as pltpu
from jax.sharding import Mesh
from jax.sharding import PartitionSpec as P

EP = ("z", "x")
TP = ("y", "c")
NX = 4
CAP = 32
SEATS = 64
ROWS = NX * CAP
F32 = jnp.float32
BF16 = jnp.bfloat16
DY, XT, META = 0, 1, 2


def dot(a, b, ca=1, cb=0):
    return lax.dot_general(a, b, (((ca,), (cb,)), ((), ())), preferred_element_type=F32)


def kernel(
    nz, ids_hbm, rw_hbm, tok_hbm, cot_hbm, gate_hbm, up_hbm, down_hbm, sg_hbm, su_hbm,
    tg_hbm, rg_hbm, gg_hbm, ug_hbm, dg_hbm,
    ids_ref, rw_ref, tok_ref, cot_ref, gate, up, down, sg, su,
    tg_ref, rg_ref, gg_ref, ug_ref, dg_ref, pre_u, pre_g, hid, hw, pw, gmat,
    sz, szm, rz, rzm, rx, rxm, perm, wcol, slots,
    zp, zr, rss, rsr, zf, du, dg, ts, tsm, cx, cxm, bs, bsm, br, brm,
    lsem, osem, zss, zrs, xss, xrs, xtr, pss, prs, rcs, rcr, acs, acr, qss, qrs, vss, vrs, wss, wrs,
):
    zi, xi, yi, ci = (lax.axis_index(a) for a in ("z", "x", "y", "c"))
    ny = nz
    part_n = nz // 2
    hf = zf.shape[-1]
    tokens = tok_ref.shape[0]
    left_half = lax.div(xi, 2) == 0
    my_row = 2 * lax.rem(xi, 2)
    seat0 = pl.multiple_of(SEATS * lax.div(xi, 2), SEATS)

    def near_first(k):
        k = jnp.int32(k)
        return jnp.where(lax.rem(k, 2) == 1, lax.div(k + 1, 2), nz - lax.div(k, 2))

    def came(k):
        return lax.rem(zi + 2 * nz - near_first(k), nz)

    def remote(src, dst, ssem, rsem, **where):
        return pltpu.make_async_remote_copy(
            src_ref=src, dst_ref=dst, send_sem=ssem, recv_sem=rsem,
            device_id=where, device_id_type=pl.DeviceIdType.MESH,
        )

    barrier = pltpu.get_barrier_semaphore()

    def greet(**where):
        pl.semaphore_signal(barrier, 1, device_id=where, device_id_type=pl.DeviceIdType.MESH)

    for k in range(1, nz):
        greet(z=lax.rem(zi + k, nz))
    for k in range(1, NX):
        greet(x=lax.rem(xi + k, NX))
    greet(y=lax.rem(yi + 1, ny))
    greet(y=lax.rem(yi + ny - 1, ny))
    greet(c=1 - ci)

    loads = [
        pltpu.make_async_copy(src, dst, lsem.at[i])
        for i, (src, dst) in enumerate(
            (
                (ids_hbm, ids_ref), (rw_hbm, rw_ref), (cot_hbm, cot_ref), (tok_hbm, tok_ref),
                (down_hbm, down), (sg_hbm, sg), (su_hbm, su), (gate_hbm, gate), (up_hbm, up),
            )
        )
    ]
    results = [
        pltpu.make_async_copy(src, dst, osem.at[i])
        for i, (src, dst) in enumerate(
            (
                (tg_ref, tg_hbm), (rg_ref, rg_hbm), (gg_ref, gg_hbm),
                (ug_ref, ug_hbm), (dg_ref, dg_hbm),
            )
        )
    ]
    for copy in loads:
        copy.start()
    loads[0].wait()
    loads[1].wait()

    experts, groups = 4 * 2 * nz, 2 * nz
    id0, id1 = ids_ref[0:1, :], ids_ref[1:2, :]
    rw0, rw1 = rw_ref[0:1, :], rw_ref[1:2, :]
    group = lax.shift_right_logical(id0, 2)
    erow = lax.broadcasted_iota(jnp.int32, (experts, tokens), 0)
    hot0, hot1 = erow == id0, erow == id1
    chosen = jnp.where(hot0, 1.0, 0.0) + jnp.where(hot1, 1.0, 0.0)
    grow = lax.broadcasted_iota(jnp.int32, (groups, tokens), 0)
    ingroup = jnp.where(grow == group, 1.0, 0.0)
    earlier = jnp.where(
        lax.broadcasted_iota(jnp.int32, (tokens, tokens), 0)
        < lax.broadcasted_iota(jnp.int32, (tokens, tokens), 1),
        1.0, 0.0,
    ).astype(BF16)
    count = dot(jnp.concatenate([chosen, ingroup], axis=0).astype(BF16), earlier)
    rank = jnp.sum(ingroup * count[experts:], axis=0, keepdims=True)
    target = group * SEATS + rank.astype(jnp.int32)
    weight = jnp.where(hot0, rw0, 0.0) + jnp.where(hot1, rw1, 0.0)
    weight_hi = weight.astype(BF16).astype(F32)
    pw[0] = chosen * (count[:experts] + 1.0)
    pw[1] = weight_hi
    pw[2] = weight - weight_hi

    def seat_rows(zt):
        row = lax.broadcasted_iota(jnp.int32, (2 * SEATS, tokens), 0) + zt * (2 * SEATS)
        return jnp.where(row == target, 1.0, 0.0).astype(BF16)

    def gathered(zt):
        g = seat_rows(zt)
        gmat[pl.ds(pl.multiple_of(zt * 2 * SEATS, 2 * SEATS), 2 * SEATS), :] = g
        e0 = pl.multiple_of(zt * 8, 8)
        lhs = jnp.concatenate([pw[i, pl.ds(e0, 8), :] for i in range(3)], axis=0).astype(BF16)
        r = dot(lhs, g, 1, 1)
        tile = jnp.concatenate(
            [r[0:4] + r[4:8], (r[8:12] + r[12:16]) + (r[16:20] + r[20:24])], axis=0
        )
        return dot(g, cot_ref[...]).astype(BF16), tile

    loads[2].wait()
    rows, tile = gathered(zi)
    rz[DY, zi] = rows
    rzm[zi] = tile

    def z_copy(which, zt, zs):
        if which == META:
            return remote(szm.at[zt], rzm.at[zs], zss.at[META], zrs.at[META, zs], z=zt)
        return remote(sz.at[which, zt], rz.at[which, zs], zss.at[which], zrs.at[which, zs], z=zt)

    def x_copy(which, q, xt, xs):
        if which == META:
            return remote(rzm.at[q], rxm.at[q, xs], xss.at[META], xrs.at[1, q], x=xt)
        seats = pl.ds(pl.multiple_of(SEATS * lax.div(xt, 2), SEATS), SEATS)
        return remote(
            rz.at[which, q, seats], rx.at[which, q, xs],
            xss.at[which], xtr.at[0] if which == XT else xrs.at[0, q], x=xt,
        )

    def spread(which, q):
        for d in range(1, NX):
            x_copy(which, q, lax.rem(xi + d, NX), xi).start()

    def pass_dy(q):
        spread(META, q)
        spread(DY, q)
        rx[DY, q, xi] = rz[DY, q, pl.ds(seat0, SEATS), :]
        rxm[q, xi] = rzm[q]

    def send_dy(k, _):
        zt = lax.rem(zi + near_first(k), nz)
        rows, tile = gathered(zt)
        szm[zt] = tile
        sz[DY, zt] = rows
        z_copy(META, zt, zi).start()
        z_copy(DY, zt, zi).start()
        return 0

    pl.semaphore_wait(barrier, (nz - 1) + (NX - 1) + 3)

    lax.fori_loop(1, nz, send_dy, 0)
    pass_dy(zi)

    def rows_of_tokens(zt):
        g = gmat[pl.ds(pl.multiple_of(zt * 2 * SEATS, 2 * SEATS), 2 * SEATS), :]
        return dot(g, tok_ref[...]).astype(BF16)

    def send_x(k, _):
        zt = lax.rem(zi + near_first(k), nz)
        sz[XT, zt] = rows_of_tokens(zt)
        z_copy(XT, zt, zi).start()
        return 0

    def elementwise(i, _):
        q, j = lax.div(i, 2), lax.rem(i, 2)
        g = sg[pl.ds(NX * q, NX), j].astype(F32).reshape(ROWS, -1)
        u = su[pl.ds(NX * q, NX), j].astype(F32).reshape(ROWS, -1)
        s = jax.nn.sigmoid(g)
        gs = g * s
        pre_u[j, q] = gs
        pre_g[j, q] = u * s * (1.0 + g * (1.0 - s))
        hid[j, q] = gs * u
        return 0

    def take_dy(k):
        q = came(k)
        z_copy(META, q, q).wait_recv()
        z_copy(DY, q, q).wait_recv()
        pass_dy(q)

    def pair_copy(q, h):
        return remote(zp.at[q, 1 - ci], zr.at[q], pss.at[0], prs.at[h], c=1 - ci)

    def back_partial(k):
        q = came(k)
        metas, rows = rxm.at[q, pl.ds(0, NX - 1)], rx.at[DY, q, pl.ds(0, NX - 1)]
        remote(metas, metas, xss.at[META], xrs.at[1, q], c=1 - ci).wait_recv()
        remote(rows, rows, xss.at[DY], xrs.at[0, q], c=1 - ci).wait_recv()
        t = rxm[q]
        t = jnp.where(left_half, t[:, :, :SEATS], t[:, :, SEATS:])
        line = lax.broadcasted_iota(jnp.int32, t.shape, 1)

        def lanes(i):
            v = jnp.sum(jnp.where(line == i, t, 0.0), axis=1)
            return jnp.concatenate([v[n : n + 1] for n in range(NX)], axis=1)

        base = CAP * lax.div(lax.broadcasted_iota(jnp.int32, (1, NX * SEATS), 1), SEATS)
        slot = lax.broadcasted_iota(jnp.int32, (ROWS, NX * SEATS), 0)
        for j in range(2):
            place = lanes(my_row + j).astype(jnp.int32)
            key = jnp.where(place > 0, place - 1 + base, -1)
            hit = slot == key
            perm[q, pl.ds(j * ROWS, ROWS), :] = jnp.where(hit, 1.0, 0.0).astype(BF16)
            w = jnp.sum(jnp.where(hit, lanes(4 + my_row + j), 0.0), axis=1, keepdims=True)
            wcol[j, q] = jnp.broadcast_to(w, (ROWS, 128))
        arrived = rx[DY, q].reshape(NX * SEATS, -1)
        moved = dot(perm[q], arrived).astype(BF16)
        for j in range(2):
            part = moved[j * ROWS : (j + 1) * ROWS]
            slots[DY, j, q] = part
            z = dot(part, down[j], 1, 1).astype(BF16)
            zp[q, 0, j] = z[:, :hf]
            zp[q, 1, j] = z[:, hf:]
        pair_copy(q, k // part_n).start()

    piece = ROWS // 2
    half_y = ny // 2
    hops = {
        (0, 0): half_y, (0, 1): ny - 1 - half_y, (1, 0): ny - 1 - half_y, (1, 1): half_y,
    }
    flows = list(hops)

    def at_y(d):
        return lax.rem(yi + d + 2 * ny, ny)

    def unit(h, d):
        return came(part_n * h + lax.div(d, 2)), lax.rem(d, 2)

    def own(h, d, p):
        q, j = unit(h, d)
        rows = pl.ds(p * piece, piece)
        return zp[q, ci, j, rows, :].astype(F32) + zr[q, j, rows, :].astype(F32)

    def rs_copy(h, p, way, s):
        return remote(
            rss.at[h, p, way, s - 1], rsr.at[h, p, way, s - 1],
            rcs.at[h, p, way], rcr.at[h, p, way, s - 1], y=at_y(1 - 2 * way),
        )

    def rs_step(h, s):
        for p, way in flows:
            if s > hops[p, way]:
                continue
            total = own(h, at_y((1 - 2 * way) * (hops[p, way] + 1 - s)), p)
            if s > 1:
                rs_copy(h, p, way, s - 1).wait_recv()
                total = total + rsr[h, p, way, s - 2].astype(F32)
            rss[h, p, way, s - 1] = total.astype(BF16)
            rs_copy(h, p, way, s).start()

    def ag_copy(h, p, way, s):
        step = 1 - 2 * way
        q, j = unit(h, at_y(-step * (s - 1)))
        spot = zf.at[q, ci, j, pl.ds(p * piece, piece)]
        return remote(
            spot, spot, acs.at[h, p, way], acr.at[h, p, way, s - 1], y=at_y(step)
        )

    def ag_wait(h, p, way, s):
        q, j = unit(h, at_y(-(1 - 2 * way) * s))
        spot = zf.at[q, ci, j, pl.ds(p * piece, piece)]
        remote(
            spot, spot, acs.at[h, p, way], acr.at[h, p, way, s - 1], y=at_y(1)
        ).wait_recv()

    def half_copy(q, j, c):
        spot = zf.at[q, c, j]
        return remote(spot, spot, qss.at[0], qrs.at[q], c=1 - ci)

    def rs_end(h):
        q, j = unit(h, yi)
        for p in range(2):
            total = own(h, yi, p)
            for way in range(2):
                if hops[p, way] > 0:
                    rs_copy(h, p, way, hops[p, way]).wait_recv()
                    total = total + rsr[h, p, way, hops[p, way] - 1].astype(F32)
            zf[q, ci, j, pl.ds(p * piece, piece), :] = total.astype(BF16)
        for p, way in flows:
            if hops[p, way] > 0:
                ag_copy(h, p, way, 1).start()
        half_copy(q, j, ci).start()

    def ag_step(h, s):
        for p, way in flows:
            if s > hops[p, way]:
                continue
            ag_wait(h, p, way, s)
            if s + 1 <= hops[p, way]:
                ag_copy(h, p, way, s + 1).start()
        for d in (-s, s) if 2 * s < ny else (s,):
            q, j = unit(h, at_y(d))
            half_copy(q, j, ci).start()

    def take_x(k):
        q = came(k)
        if not (isinstance(k, int) and k == 0):
            z_copy(XT, q, q).wait_recv()
        spread(XT, q)
        rx[XT, q, xi] = rz[XT, q, pl.ds(seat0, SEATS), :]

    def back_copy(q, xt, xs):
        return remote(ts.at[q, xt], cx.at[q, xs], vss.at[0], vrs.at[0, q], x=xt)

    def back_meta(q, xt, xs):
        return remote(tsm.at[q, xt], cxm.at[q, xs], vss.at[1], vrs.at[1, q], x=xt)

    def consume(q):
        both = zf.at[q, 1 - ci]
        remote(both, both, qss.at[0], qrs.at[q], c=1 - ci).wait_recv()
        grads, tiles = [], None
        line = lax.broadcasted_iota(jnp.int32, (8, 2 * SEATS), 0)
        side = lax.div(lax.broadcasted_iota(jnp.int32, (8, 2 * SEATS), 1), SEATS) == lax.div(xi, 2)
        for j in range(2):
            z = jnp.concatenate([zf[q, 0, j], zf[q, 1, j]], axis=1).astype(F32)
            w = jnp.concatenate([wcol[j, q]] * (z.shape[-1] // 128), axis=1)
            wz = w * z
            up_grad = (wz * pre_u[j, q]).astype(BF16)
            gate_grad = (wz * pre_g[j, q]).astype(BF16)
            du[j, q] = up_grad
            dg[j, q] = gate_grad
            hb = hid[j, q].astype(BF16).astype(F32)
            score = jnp.sum(hb * z, axis=1, keepdims=True)
            p = perm[q, pl.ds(j * ROWS, ROWS), :].astype(F32)
            seat_score = jnp.sum(p * score, axis=0, keepdims=True)
            s = dot(gate_grad, gate[j], 1, 1) + dot(up_grad, up[j], 1, 1)
            grads.append(s.astype(BF16))
            mask = side & (line == my_row + j)
            made = []
            for n in range(NX):
                one = seat_score[:, n * SEATS : (n + 1) * SEATS]
                made.append(jnp.where(mask, jnp.concatenate([one, one], axis=1), 0.0))
            tiles = made if tiles is None else [a + b for a, b in zip(tiles, made)]
        for n in range(NX):
            tsm[q, n] = tiles[n]
        t = dot(perm[q], jnp.concatenate(grads, axis=0), 0, 0).astype(BF16)
        ts[q] = t.reshape(NX, SEATS, -1)
        for d in range(1, NX):
            xt = lax.rem(xi + d, NX)
            back_meta(q, xt, xi).start()
            back_copy(q, xt, xi).start()
        cx[q, xi] = ts[q, xi]
        cxm[q, xi] = tsm[q, xi]

    def home_copy(q, zs):
        return remote(bs.at[q], br.at[zs], wss.at[0], wrs.at[0], z=q)

    def home_meta(q, zs):
        return remote(bsm.at[q], brm.at[zs], wss.at[1], wrs.at[1], z=q)

    def combine(q):
        metas, rows = cxm.at[q, pl.ds(0, NX - 1)], cx.at[q, pl.ds(0, NX - 1)]
        remote(metas, metas, vss.at[1], vrs.at[1, q], c=1 - ci).wait_recv()
        remote(rows, rows, vss.at[0], vrs.at[0, q], c=1 - ci).wait_recv()
        first = (cx[q, 0].astype(F32) + cx[q, 1].astype(F32)).astype(BF16)
        second = (cx[q, 2].astype(F32) + cx[q, 3].astype(F32)).astype(BF16)
        scores = (cxm[q, 0] + cxm[q, 1]) + (cxm[q, 2] + cxm[q, 3])

        @pl.when(q == zi)
        def _():
            br[q, pl.ds(0, SEATS), :] = first
            br[q, pl.ds(SEATS, SEATS), :] = second
            brm[q] = scores

        @pl.when(q != zi)
        def _():
            bs[q, pl.ds(0, SEATS), :] = first
            bs[q, pl.ds(SEATS, SEATS), :] = second
            bsm[q] = scores
            home_meta(q, zi).start()
            home_copy(q, zi).start()

    def turn(h, i):
        d = (i + 1) // 2
        even = lax.rem(yi, 2) == 0
        shift = jnp.where(even, d, -d) if i % 2 == 0 else jnp.where(even, -d, d)
        return came(part_n * h + lax.rem(lax.div(yi, 2) + shift + 2 * part_n, part_n))

    def down_grads(j):
        def weigh(q, _):
            w = jnp.concatenate([wcol[j, q]] * (hid.shape[-1] // 128), axis=1)
            hw[j, q] = (w * hid[j, q]).astype(BF16)
            return 0

        lax.fori_loop(0, nz, weigh, 0)
        weighted = hw[j].reshape(nz * ROWS, -1)
        dy = slots[DY, j].reshape(nz * ROWS, -1)
        dg_ref[j] = dot(weighted, dy, 0, 0).astype(BF16)

    def wait_pairs(h):
        span = zr.at[pl.ds(0, part_n)]
        remote(span, span, pss.at[0], prs.at[h], c=1 - ci).wait_recv()

    loads[5].wait()
    loads[6].wait()
    lax.fori_loop(0, 2 * nz, elementwise, 0)

    loads[4].wait()
    for k in range(1, part_n):
        take_dy(k)
        back_partial(k - 1)
    back_partial(part_n - 1)

    wait_pairs(0)
    rs_step(0, 1)
    for k in range(part_n, nz):
        take_dy(k)
    loads[3].wait()
    lax.fori_loop(1, nz, send_x, 0)
    rz[XT, zi] = rows_of_tokens(zi)
    backs = list(range(part_n, nz))
    for s in range(2, half_y):
        rs_step(0, s)
        for _ in range(2):
            if backs:
                back_partial(backs.pop(0))
    while backs:
        back_partial(backs.pop(0))
    if half_y > 1:
        rs_step(0, half_y)
    wait_pairs(1)
    rs_step(1, 1)
    rs_end(0)
    loads[7].wait()
    loads[8].wait()
    for s in range(2, half_y + 1):
        rs_step(1, s)
        ag_step(0, s - 1)
        if s == 2:
            for k in range(part_n):
                take_x(k)
            down_grads(0)
        else:
            consume(turn(0, s - 3))
            down_grads(1) if s == 3 else None
    rs_end(1)
    for k in range(part_n if half_y > 1 else 0, nz):
        take_x(k)
    if half_y < 2:
        down_grads(0)
    if half_y < 3:
        down_grads(1)
    results[4].start()
    ag_step(0, half_y)
    for i in range(max(half_y - 2, 0), part_n):
        consume(turn(0, i))
    for s in range(1, half_y + 1):
        ag_step(1, s)
        if s > 1:
            consume(turn(1, s - 2))
        combine(turn(0, s - 1))
    consume(turn(1, part_n - 1))
    for i in range(part_n):
        combine(turn(1, i))

    def seat_x(q, _):
        moved = dot(perm[q], rx[XT, q].reshape(NX * SEATS, -1)).astype(BF16)
        slots[XT, 0, q] = moved[:ROWS]
        slots[XT, 1, q] = moved[ROWS:]
        return 0

    x_rows = rx.at[XT, pl.ds(0, nz), pl.ds(0, NX - 1)]
    remote(x_rows, x_rows, xss.at[XT], xtr.at[0], c=1 - ci).wait_recv()
    lax.fori_loop(0, nz, seat_x, 0)

    def weight_grads(j, _):
        x = slots[XT, j].reshape(nz * ROWS, -1)
        gg_ref[j] = dot(x, dg[j].reshape(nz * ROWS, -1), 0, 0).astype(BF16)
        ug_ref[j] = dot(x, du[j].reshape(nz * ROWS, -1), 0, 0).astype(BF16)
        return 0

    lax.fori_loop(0, 2, weight_grads, 0)
    results[2].start()
    results[3].start()

    def gone(span, sem):
        remote(span, span, sem, sem, c=1 - ci).wait_send()

    def came_in(span, sem):
        remote(span, span, sem, sem, c=1 - ci).wait_recv()

    gone(szm.at[pl.ds(0, nz - 1)], zss.at[META])
    gone(rxm.at[pl.ds(0, nz), pl.ds(0, NX - 1)], xss.at[META])
    for which in (DY, XT):
        gone(sz.at[which, pl.ds(0, nz - 1)], zss.at[which])
        gone(rx.at[which, pl.ds(0, nz), pl.ds(0, NX - 1)], xss.at[which])
    gone(ts.at[pl.ds(0, nz), pl.ds(0, NX - 1)], vss.at[0])
    gone(tsm.at[pl.ds(0, nz), pl.ds(0, NX - 1)], vss.at[1])
    gone(zr, pss.at[0])
    gone(zr, qss.at[0])
    for h in range(2):
        for p, way in flows:
            if hops[p, way] > 0:
                gone(rss.at[h, p, way, pl.ds(0, hops[p, way])], rcs.at[h, p, way])
                gone(rss.at[h, p, way, pl.ds(0, hops[p, way])], acs.at[h, p, way])

    came_in(brm.at[pl.ds(0, nz - 1)], wrs.at[1])
    came_in(br.at[pl.ds(0, nz - 1)], wrs.at[0])
    tg_ref[...] = dot(gmat[...], br[...].reshape(nz * 2 * SEATS, -1), 0, 0).astype(BF16)
    results[0].start()
    scores = jnp.concatenate([brm[q] for q in range(nz)], axis=1)
    hi = scores.astype(BF16)
    rest1 = scores - hi.astype(F32)
    mid = rest1.astype(BF16)
    low = (rest1 - mid.astype(F32)).astype(BF16)
    g = gmat[...]
    picked = dot(hi, g) + dot(mid, g) + dot(low, g)
    line = lax.broadcasted_iota(jnp.int32, picked.shape, 0)
    rg_ref[0:1, :] = jnp.sum(jnp.where(line == (id0 & 3), picked, 0.0), axis=0, keepdims=True)
    rg_ref[1:2, :] = jnp.sum(jnp.where(line == (id1 & 3), picked, 0.0), axis=0, keepdims=True)
    results[1].start()

    gone(bsm.at[pl.ds(0, nz - 1)], wss.at[1])
    gone(bs.at[pl.ds(0, nz - 1)], wss.at[0])
    for copy in results:
        copy.wait()


def forward(*refs):
    n = 5
    froms, tos, held = refs[:n], refs[n : 2 * n], refs[2 * n : 3 * n]
    came, gone = refs[3 * n :]
    ins = [pltpu.make_async_copy(froms[i], held[i], came.at[i]) for i in range(n)]
    outs = [pltpu.make_async_copy(held[i], tos[i], gone.at[i]) for i in range(n)]
    for copy in ins:
        copy.start()
    for i in range(n):
        ins[i].wait()
        outs[i].start()
    for copy in outs:
        copy.wait()


def local(nz, ids, rw, tok, cot, gate, up, down, sg, su):
    tokens, wide = tok.shape
    f = gate.shape[-1]
    hf = f // 2
    ny = nz
    experts = 8 * nz
    vm = pltpu.VMEM
    dma = pltpu.SemaphoreType.DMA
    steps = max(ny // 2, 1)
    piece = ROWS // 2
    shapes = (
        jax.ShapeDtypeStruct(tok.shape, BF16),
        jax.ShapeDtypeStruct((2, tokens), F32),
        jax.ShapeDtypeStruct(gate.shape, BF16),
        jax.ShapeDtypeStruct(up.shape, BF16),
        jax.ShapeDtypeStruct(down.shape, BF16),
    )
    held = [vm(s.shape, s.dtype) for s in shapes]
    scratch = [
        vm((2, tokens), jnp.int32), vm((2, tokens), F32), vm(tok.shape, BF16), vm(cot.shape, BF16),
        vm(gate.shape, BF16), vm(up.shape, BF16), vm(down.shape, BF16),
        vm(sg.shape, BF16), vm(su.shape, BF16), *held,
        vm((2, nz, ROWS, f), F32), vm((2, nz, ROWS, f), F32), vm((2, nz, ROWS, f), F32),
        vm((2, nz, ROWS, f), BF16),
        vm((3, experts, tokens), F32), vm((nz * 2 * SEATS, tokens), BF16),
        vm((2, nz, 2 * SEATS, wide), BF16), vm((nz, 8, 128), F32),
        vm((2, nz, 2 * SEATS, wide), BF16), vm((nz, 8, 128), F32),
        vm((2, nz, NX, SEATS, wide), BF16), vm((nz, NX, 8, 128), F32),
        vm((nz, 2 * ROWS, NX * SEATS), BF16), vm((2, nz, ROWS, 128), F32),
        vm((2, 2, nz, ROWS, wide), BF16),
        vm((nz, 2, 2, ROWS, hf), BF16), vm((nz, 2, ROWS, hf), BF16),
        vm((2, 2, 2, steps, piece, hf), BF16), vm((2, 2, 2, steps, piece, hf), BF16),
        vm((nz, 2, 2, ROWS, hf), BF16),
        vm((2, nz, ROWS, f), BF16), vm((2, nz, ROWS, f), BF16),
        vm((nz, NX, SEATS, wide), BF16), vm((nz, NX, 8, 128), F32),
        vm((nz, NX, SEATS, wide), BF16), vm((nz, NX, 8, 128), F32),
        vm((nz, 2 * SEATS, wide), BF16), vm((nz, 8, 128), F32),
        vm((nz, 2 * SEATS, wide), BF16), vm((nz, 8, 128), F32),
        dma((9,)), dma((5,)), dma((3,)), dma((3, nz)), dma((3,)), dma((2, nz)), dma((1,)),
        dma((1,)), dma((2,)), dma((2, 2, 2)), dma((2, 2, 2, steps)),
        dma((2, 2, 2)), dma((2, 2, 2, steps)), dma((1,)), dma((nz,)),
        dma((2,)), dma((2, nz)), dma((2,)), dma((2,)),
    ]
    outside = pl.BlockSpec(memory_space=pl.ANY)
    made = pl.pallas_call(
        functools.partial(kernel, nz),
        out_shape=shapes,
        in_specs=[outside] * 9,
        out_specs=(outside,) * 5,
        scratch_shapes=scratch,
        compiler_params=pltpu.CompilerParams(
            collective_id=0, has_side_effects=True, vmem_limit_bytes=60 * 1024 * 1024
        ),
    )(ids.T, rw.T, tok, cot, gate, up, down, sg, su)
    out = pl.pallas_call(
        forward,
        out_shape=shapes,
        in_specs=[outside] * 5,
        out_specs=(outside,) * 5,
        scratch_shapes=[*held, dma((5,)), dma((5,))],
        compiler_params=pltpu.CompilerParams(vmem_limit_bytes=60 * 1024 * 1024),
    )(*made)
    return (out[0], out[1].T, *out[2:])


def on_axes(mesh, nz):
    return jax.shard_map(
        functools.partial(
            lambda n, tok, cot, ids, rw, *others: local(n, ids, rw, tok, cot, *others), nz
        ),
        mesh=mesh,
        in_specs=(
            P(EP, TP), P(EP, TP), P(EP, None), P(EP, None),
            P(EP, TP, None), P(EP, TP, None), P(EP, None, TP),
            P(None, EP, None, None), P(None, EP, None, None),
        ),
        out_specs=(
            P(EP, TP), P(EP, None), P(EP, TP, None), P(EP, TP, None), P(EP, None, TP),
        ),
        check_vma=False,
    )


def solution(mesh):
    nz = mesh.shape["ep"] // NX
    return on_axes(Mesh(mesh.devices.reshape(nz, NX, nz, 2), ("z", "x", "y", "c")), nz)
```

time: 104 us -> 93.2 us (0.90)
  the two profiles are of different devices: /device:TPU:16 before, /device:TPU:1 now
where the time goes in v2:
time: 93.2 us; the launch traced here: 91.8 us
  Pallas kernels  91.1 us (98%)
    pallas_call x1, Pallas kernels, local(): pl.pallas_call(functools.partial(kernel, nz), out_shape=shapes, in_specs=...  88.8 us
    pallas_call x1, Pallas kernels, local(): pl.pallas_call(forward, out_shape=shapes, in_specs=[outside] * 5, out_spe...  2.35 us

profile of v2, /device:TPU:1, one launch (start us, length us, event | category | flops | bytes accessed | tf_op | source)
XLA Modules:
  0.0 91.8 jit_solution(7759844205264032879)
XLA Ops:
  0.6 88.8 %shard_map.128 = (bf16[512,256]{1,0:T(8,128)(2,1)}, f32[2,512]{1,0:T(2,128)}, bf16[2,256,512]{2,1,0:T(8,128)(2,1)}, bf16[2,256,512]{2,1,0:T(8,128)(2,1)}, bf16[2,512,256]{2,1,0:T(8,128)(2,1)}) custom-call(s32[2,512]{1,0:T(2,128)} %bitcast.3, f32[2,512]{1,0:T(2,128)} %bitcast.4, bf16[512,256]{1,0:T(8,128)(2,1)} %tok_hbm.1, bf16[512,256]{1,0:T(8,128)(2,1)} %cot_hbm.1, ...), custom_call_target="tpu_custom_call" | custom-call | tf_op jit(solution)/shard_map/pallas_call | solution.py:598
  89.4 2.4 %shard_map.129 = (bf16[512,256]{1,0:T(8,128)(2,1)}, f32[2,512]{1,0:T(2,128)}, bf16[2,256,512]{2,1,0:T(8,128)(2,1)}, bf16[2,256,512]{2,1,0:T(8,128)(2,1)}, bf16[2,512,256]{2,1,0:T(8,128)(2,1)}) custom-call(bf16[512,256]{1,0:T(8,128)(2,1)} %get-tuple-element.15.refs_0_, f32[2,512]{1,0:T(2,128)} %get-tuple-element.16.refs_1_, ...), custom_call_target="tpu_custom_call" | custom-call | tf_op jit(solution)/shard_map/pallas_call | solution.py:608
